TPU v7x, 32 devices: a whole 2x2x4 slice. The times are simulated.
32 devices in a mesh: kv: 8 (over z, x), tp: 4 (over y, core).
Axes of the slice: x: 2, y: 2, z: 4, core: 2. Of those that a mesh axis runs over, the one named last changes fastest.
Arguments:
- tokens: bfloat16 [4, 4096], P(None, 'kv'), may hold values from -30 to 30
- norm_gain: float32 [4096], P('kv'), may hold values from 0.1 to 1.9
- query_weight: bfloat16 [4096, 2048], P('kv', 'tp'), may hold values from -0.09375 to 0.09375
- cache_keys: bfloat16 [4, 4096, 16, 128], P(None, 'kv', 'tp'), may hold values from -180 to 180
- cache_values: bfloat16 [4, 4096, 16, 128], P(None, 'kv', 'tp'), may hold values from -6 to 6
- lengths: int32 [4], replicated, may hold values from 2049 to 4096, as said below
- lambdas: float32 [16], P('tp'), may hold values from 0.3 to 0.8
- head_gain: float32 [128], replicated, may hold values from 0.1 to 1.9
- out_weight: bfloat16 [2048, 4096], P('tp', 'kv'), may hold values from -0.125 to 0.125
Outputs:
- mixed: bfloat16 [4, 4096], P(None, 'kv')
Inputs may be any that keep to these rules, and one draw needn't show every extreme that they name: `lengths`: every length is more than half of 4096; some sequence has exactly 4096.
All inputs are finite; a program needn't handle non-finite values.
Results may differ from a plain program's by a relative error of at most 0.02.
Values may be sent and summed in bfloat16 or wider, within the bound.
No kernel may reach another device: no remote copies, remote signals or barrier semaphores. Data moves between devices by JAX's collectives and lax.ppermute only.
A program may use at most 64 MiB of HBM per device.

v0:
```python
import jax
import jax.numpy as jnp
from jax import lax
from jax.sharding import PartitionSpec as P

D = 4096
HD = 64
VD = 128
eps = 1e-06
NEG = -1e30


def body(
    tokens,
    norm_gain,
    query_weight,
    cache_keys,
    cache_values,
    lengths,
    lambdas,
    head_gain,
    out_weight,
):
    seqs = tokens.shape[0]
    span = cache_keys.shape[1]
    local_heads = cache_keys.shape[2]
    floats = tokens.astype(jnp.float32)
    squares = jnp.sum(floats * floats, axis=1)
    scaled_logits = (floats * norm_gain).astype(jnp.bfloat16)
    partial_value = jnp.dot(scaled_logits, query_weight, preferred_element_type=jnp.float32)
    total_squares, projected = lax.psum((squares, partial_value), "kv")
    inverse = lax.rsqrt(total_squares / D + eps)
    query = (
        (projected * inverse[:, None] * 0.125)
        .astype(jnp.bfloat16)
        .reshape(seqs, local_heads, 2, HD)
    )
    keys = cache_keys.reshape(seqs, span, local_heads, 2, HD)
    score_matrix = jnp.einsum("bhmd,bphmd->bhmp", query, keys, preferred_element_type=jnp.float32)
    position_indices = lax.axis_index("kv") * span + jnp.arange(span, dtype=jnp.int32)
    valid = (position_indices[None, :] < lengths[:, None])[:, None, None, :]
    score_matrix = jnp.where(valid, score_matrix, NEG)
    peak = jnp.max(score_matrix, axis=-1)
    weights = jnp.where(valid, jnp.exp(score_matrix - peak[..., None]), 0.0)
    mass = jnp.sum(weights, axis=-1)
    summed = jnp.einsum(
        "bhmp,bphv->bhmv",
        weights.astype(jnp.bfloat16),
        cache_values,
        preferred_element_type=jnp.float32,
    )
    scales = lambdas[None, :, None]
    whole_peak = lax.pmax(peak, "kv")
    factor = jnp.exp(peak - whole_peak)
    whole_mass = lax.psum(mass * factor, "kv")
    shares = factor / whole_mass
    local_part = (
        summed[:, :, 0] * shares[:, :, 0, None] - scales * summed[:, :, 1] * shares[:, :, 1, None]
    )
    attended = lax.psum(local_part, "kv")
    normed = (
        attended
        * lax.rsqrt(jnp.mean(attended * attended, axis=-1, keepdims=True) + eps)
        * head_gain
        * 0.8
    )
    normed = normed.astype(jnp.bfloat16).reshape(seqs, local_heads * VD)
    part = jnp.dot(normed, out_weight, preferred_element_type=jnp.float32).astype(jnp.bfloat16)
    return lax.psum(part, "tp").astype(jnp.float32).astype(jnp.bfloat16)


def solution(mesh):
    in_specs = (
        P(None, "kv"),
        P("kv"),
        P("kv", "tp"),
        P(None, "kv", "tp", None),
        P(None, "kv", "tp", None),
        P(),
        P("tp"),
        P(),
        P("tp", "kv"),
    )
    out_specs = P(None, "kv")
    return jax.shard_map(body, mesh=mesh, in_specs=in_specs, out_specs=out_specs, check_vma=False)
```

profile of v0, /device:TPU:0, one launch (start us, length us, event | category | flops | bytes accessed | tf_op | source)
XLA Modules:
  0.0 94.3 jit_solution(17817469448406255703)
XLA Ops:
  0.0 0.0 copy-start
  0.0 1.4 %fusion.7 = f32[4,512]{1,0:T(4,128)S(1)} fusion(bf16[512,512]{1,0:T(8,128)(2,1)} %param.11, bf16[4,512]{1,0:T(4,128)(2,1)} %param.9, f32[512]{0:T(512)} %param.10), kind=kOutput, calls=%fused_computation.19 | convolution fusion | flops 2103296 | bytes 538624 | tf_op jit(solution)/shard_map/dot_general | solution.py:30
  1.4 0.8 fusion.5
  2.2 23.6 %all-reduce = (f32[4,512]{1,0:T(4,128)S(1)}, f32[4]{0:T(128)S(1)}) all-reduce(f32[4,512]{1,0:T(4,128)S(1)} %fusion.7, f32[4]{0:T(128)S(1)} %fusion.5), channel_id=1, replica_groups=mesh['kv'=8,'tp'=4] {'kv'}, use_global_device_ids=true, to_apply=%region_0.0 | all-reduce | flops 2052 | bytes 16416 | tf_op jit(solution)/shard_map/psum | solution.py:31
  25.8 0.1 multiply_convert_fusion.1
  25.9 0.1 reshape.55
  26.0 4.3 %copy.20 = bf16[4,512,4,128]{1,3,2,0:T(8,128)(2,1)} copy(bf16[4,512,4,128]{3,2,1,0:T(4,128)(2,1)} %param.12) | data formatting | bytes 4194304 | tf_op args[3]
  30.3 0.0 copy-start.3
  30.3 0.0 copy-start.2
  30.3 0.0 copy-start.4
  30.3 0.0 copy-start.1
  30.3 2.0 %fusion.16 = f32[4,4,2,1,512]{4,3,2,1,0:T(1,128)S(1)} fusion(bf16[4,4,2,64,1]{3,4,2,1,0:T(2,128)(2,1)S(1)} %reshape.55, bf16[4,512,4,2,64]{1,4,3,2,0:T(8,128)(2,1)} %bitcast.33), kind=kOutput, calls=%fused_computation.31 | convolution fusion | flops 2097152 | bytes 2166784 | tf_op jit(solution)/shard_map/bhmd,bphmd->bhmp/dot_general | solution.py:39
  32.3 0.0 copy-done.3
  32.3 0.1 broadcast_compare_fusion
  32.4 0.1 fusion.2
  32.5 0.2 fusion.14
  32.7 17.4 %pmax.7 = f32[4,4,2]{2,1,0:T(4,128)S(1)} all-reduce(f32[4,4,2]{2,1,0:T(4,128)S(1)} %fusion.2), channel_id=1, replica_groups=mesh['kv'=8,'tp'=4] {'kv'}, use_global_device_ids=true, to_apply=%region_4.5 | all-reduce | flops 32 | bytes 256 | tf_op jit(solution)/shard_map/pmax | solution.py:53
  50.1 19.4 %psum.37 = f32[4,4,2]{2,1,0:T(4,128)S(1)} all-reduce(f32[4,4,2]{2,1,0:T(4,128)S(1)} %bitcast.42), channel_id=1, replica_groups=mesh['kv'=8,'tp'=4] {'kv'}, use_global_device_ids=true, to_apply=%region_6.7 | all-reduce | flops 32 | bytes 256 | tf_op jit(solution)/shard_map/psum | solution.py:55
  69.6 0.1 slice_reduce_fusion.1
  69.7 0.0 copy-done
  69.7 0.5 fusion
  70.2 0.0 copy-done.2
  70.2 0.1 multiply_subtract_fusion
  70.3 17.4 %psum.38 = f32[4,4,128]{2,1,0:T(4,128)S(1)} all-reduce(f32[4,4,128]{2,1,0:T(4,128)S(1)} %multiply_subtract_fusion), channel_id=1, replica_groups=mesh['kv'=8,'tp'=4] {'kv'}, use_global_device_ids=true, to_apply=%region_7.8 | all-reduce | flops 2048 | bytes 16384 | tf_op jit(solution)/shard_map/psum | solution.py:60
  87.7 0.1 multiply_reduce_fusion
  87.8 0.0 copy-done.4
  87.8 0.1 fusion.6
  87.8 0.0 copy-done.1
  87.9 0.2 convolution_convert_fusion
  88.0 6.2 %psum.39 = bf16[4,512]{1,0:T(4,128)(2,1)} all-reduce(bf16[4,512]{1,0:T(4,128)(2,1)S(1)} %convolution_convert_fusion), channel_id=1, replica_groups=mesh['kv'=8,'tp'=4] {'tp'}, use_global_device_ids=true, to_apply=%region_9.10 | all-reduce | flops 2048 | bytes 8192 | tf_op jit(solution)/shard_map/psum | solution.py:69
  (6 shorter events, 0.1 us)
Async XLA Ops:
  0.0 69.7 %copy-start = (bf16[4,512,4,128]{3,2,1,0:T(4,128)(2,1)S(1)}, bf16[4,512,4,128]{3,2,1,0:T(4,128)(2,1)}, u32[]{:S(2)}) copy-start(bf16[4,512,4,128]{3,2,1,0:T(4,128)(2,1)} %param.13) | copy-start | bytes 6291460
  30.3 2.0 %copy-start.3 = (s32[4]{0:T(128)S(1)}, s32[4]{0:T(128)}, u32[]{:S(2)}) copy-start(s32[4]{0:T(128)} %param.14) | copy-start | bytes 52
  30.3 39.9 %copy-start.2 = (f32[4]{0:T(128)S(1)}, f32[4]{0:T(128)}, u32[]{:S(2)}) copy-start(f32[4]{0:T(128)} %param.15) | copy-start | bytes 52
  30.3 57.5 %copy-start.4 = (f32[128]{0:T(128)S(1)}, f32[128]{0:T(128)}, u32[]{:S(2)}) copy-start(f32[128]{0:T(128)} %param.16) | copy-start | bytes 1540
  30.3 57.6 %copy-start.1 = (bf16[512,512]{1,0:T(8,128)(2,1)S(1)}, bf16[512,512]{1,0:T(8,128)(2,1)}, u32[]{:S(2)}) copy-start(bf16[512,512]{1,0:T(8,128)(2,1)} %param.17) | copy-start | bytes 1572868
where the time goes:
time: 94.6 us; the launch traced here: 94.3 us
  blocking collectives  84 us (89%)
  local copies, waits for them, and re-layouts  4.54 us (5%)
  matrix products  4.05 us (4%)
  other arithmetic  1.59 us (2%)
    psum x1, blocking collectives, body(): total_squares, projected = lax.psum((squares, partial_value), 'kv')  23.6 us
    psum x1, blocking collectives, body(): whole_mass = lax.psum(mass * factor, 'kv')  19.4 us
    pmax x1, blocking collectives, body(): whole_peak = lax.pmax(peak, 'kv')  17.4 us
    psum x1, blocking collectives, body(): attended = lax.psum(local_part, 'kv')  17.4 us
    psum x1, blocking collectives, body(): return lax.psum(part, 'tp').astype(jnp.float32).astype(jnp.bfloat16)  6.24 us
    unnamed x11, local copies, waits for them, and re-layouts  4.29 us
    dot_general x1, matrix products, body(): jnp.einsum('bhmd,bphmd->bhmp', query, keys, preferred_element_type=jnp.fl...  2.03 us

commit v1 on v0

--- a/solution.py
+++ b/solution.py
@@ -52,7 +52,7 @@
     scales = lambdas[None, :, None]
     whole_peak = lax.pmax(peak, "kv")
     factor = jnp.exp(peak - whole_peak)
-    whole_mass = lax.psum(mass * factor, "kv")
+    whole_mass = jnp.sum(lax.all_gather(mass * factor, "kv"), axis=0)
     shares = factor / whole_mass
     local_part = (
         summed[:, :, 0] * shares[:, :, 0, None] - scales * summed[:, :, 1] * shares[:, :, 1, None]

time: 94.6 us -> 108 us (1.14)
  blocking collectives: 84 us -> 97.2 us
    all_gather x0 -> x1, blocking collectives: none -> 30.6 us  [body(): whole_mass = jnp.sum(lax.all_gather(mass * factor, 'kv'), axis=0)]
    psum x1 -> x0, blocking collectives: 19.4 us -> none  [body(): whole_mass = lax.psum(mass * factor, 'kv')]
    psum x1, blocking collectives: 17.4 us -> 19.4 us  [body(): attended = lax.psum(local_part, 'kv')]
where the time goes in v1:
time: 108 us
  blocking collectives  97.2 us (90%)
  local copies, waits for them, and re-layouts  4.76 us (4%)
  matrix products  4.05 us (4%)
  other arithmetic  1.62 us (2%)
    all_gather x1, blocking collectives, body(): whole_mass = jnp.sum(lax.all_gather(mass * factor, 'kv'), axis=0)  30.6 us
    psum x1, blocking collectives, body(): total_squares, projected = lax.psum((squares, partial_value), 'kv')  23.6 us
    psum x1, blocking collectives, body(): attended = lax.psum(local_part, 'kv')  19.4 us
    pmax x1, blocking collectives, body(): whole_peak = lax.pmax(peak, 'kv')  17.4 us
    psum x1, blocking collectives, body(): return lax.psum(part, 'tp').astype(jnp.float32).astype(jnp.bfloat16)  6.24 us
    unnamed x11, local copies, waits for them, and re-layouts  4.29 us

profile of v1, /device:TPU:0, one launch (start us, length us, event | category | flops | bytes accessed | tf_op | source)
XLA Modules:
  0.0 107.7 jit_solution(17429866928546366466)
XLA Ops:
  0.0 0.0 copy-start
  0.0 1.4 %fusion.7 = f32[4,512]{1,0:T(4,128)S(1)} fusion(bf16[512,512]{1,0:T(8,128)(2,1)} %param.11, bf16[4,512]{1,0:T(4,128)(2,1)} %param.9, f32[512]{0:T(512)} %param.10), kind=kOutput, calls=%fused_computation.19 | convolution fusion | flops 2103296 | bytes 538624 | tf_op jit(solution)/shard_map/dot_general | solution.py:30
  1.4 0.8 fusion.5
  2.2 23.6 %all-reduce = (f32[4,512]{1,0:T(4,128)S(1)}, f32[4]{0:T(128)S(1)}) all-reduce(f32[4,512]{1,0:T(4,128)S(1)} %fusion.7, f32[4]{0:T(128)S(1)} %fusion.5), channel_id=1, replica_groups=mesh['kv'=8,'tp'=4] {'kv'}, use_global_device_ids=true, to_apply=%region_0.0 | all-reduce | flops 2052 | bytes 16416 | tf_op jit(solution)/shard_map/psum | solution.py:31
  25.8 0.1 multiply_convert_fusion.1
  25.9 0.1 reshape.56
  26.0 4.3 %copy.25 = bf16[4,512,4,128]{1,3,2,0:T(8,128)(2,1)} copy(bf16[4,512,4,128]{3,2,1,0:T(4,128)(2,1)} %param.12) | data formatting | bytes 4194304 | tf_op args[3]
  30.3 0.0 copy-start.3
  30.3 0.0 copy-start.2
  30.3 0.0 copy-start.4
  30.3 0.0 copy-start.1
  30.3 2.0 %fusion.16 = f32[4,4,2,1,512]{4,3,2,1,0:T(1,128)S(1)} fusion(bf16[4,4,2,64,1]{3,4,2,1,0:T(2,128)(2,1)S(1)} %reshape.56, bf16[4,512,4,2,64]{1,4,3,2,0:T(8,128)(2,1)} %bitcast.34), kind=kOutput, calls=%fused_computation.31 | convolution fusion | flops 2097152 | bytes 2166784 | tf_op jit(solution)/shard_map/bhmd,bphmd->bhmp/dot_general | solution.py:39
  32.3 0.0 copy-done.3
  32.3 0.1 broadcast_compare_fusion
  32.4 0.1 fusion.2
  32.5 0.2 fusion.14
  32.7 17.4 %pmax.7 = f32[4,4,2]{2,1,0:T(4,128)S(1)} all-reduce(f32[4,4,2]{2,1,0:T(4,128)S(1)} %fusion.2), channel_id=1, replica_groups=mesh['kv'=8,'tp'=4] {'kv'}, use_global_device_ids=true, to_apply=%region_4.5 | all-reduce | flops 32 | bytes 256 | tf_op jit(solution)/shard_map/pmax | solution.py:53
  50.1 0.1 copy.28
  50.3 30.6 %all-gather = f32[32,4,2]{1,2,0:T(2,128)S(1)} all-gather(f32[4,4,2]{1,2,0:T(2,128)S(1)} %copy.28), channel_id=2, replica_groups=mesh['kv'=8,'tp'=4] {'kv'}, dimensions={0}, use_global_device_ids=true | all-gather | bytes 1152 | tf_op jit(solution)/shard_map/all_gather | solution.py:55
  80.9 0.1 copy.29
  81.0 0.1 slice_reduce_fusion.1
  81.2 0.0 copy-done
  81.2 0.5 fusion
  81.7 0.0 copy-done.2
  81.7 0.1 multiply_subtract_fusion
  81.7 19.4 %psum.30 = f32[4,4,128]{2,1,0:T(4,128)S(1)} all-reduce(f32[4,4,128]{2,1,0:T(4,128)S(1)} %multiply_subtract_fusion), channel_id=1, replica_groups=mesh['kv'=8,'tp'=4] {'kv'}, use_global_device_ids=true, to_apply=%region_7.8 | all-reduce | flops 2048 | bytes 16384 | tf_op jit(solution)/shard_map/psum | solution.py:60
  101.1 0.1 multiply_reduce_fusion
  101.2 0.0 copy-done.4
  101.2 0.1 fusion.6
  101.3 0.0 copy-done.1
  101.3 0.2 convolution_convert_fusion
  101.5 6.2 %psum.31 = bf16[4,512]{1,0:T(4,128)(2,1)} all-reduce(bf16[4,512]{1,0:T(4,128)(2,1)S(1)} %convolution_convert_fusion), channel_id=1, replica_groups=mesh['kv'=8,'tp'=4] {'tp'}, use_global_device_ids=true, to_apply=%region_9.10 | all-reduce | flops 2048 | bytes 8192 | tf_op jit(solution)/shard_map/psum | solution.py:69
  (7 shorter events, 0.1 us)
Async XLA Ops:
  0.0 81.2 %copy-start = (bf16[4,512,4,128]{3,2,1,0:T(4,128)(2,1)S(1)}, bf16[4,512,4,128]{3,2,1,0:T(4,128)(2,1)}, u32[]{:S(2)}) copy-start(bf16[4,512,4,128]{3,2,1,0:T(4,128)(2,1)} %param.13) | copy-start | bytes 6291460
  30.3 2.0 %copy-start.3 = (s32[4]{0:T(128)S(1)}, s32[4]{0:T(128)}, u32[]{:S(2)}) copy-start(s32[4]{0:T(128)} %param.14) | copy-start | bytes 52
  30.3 51.4 %copy-start.2 = (f32[4]{0:T(128)S(1)}, f32[4]{0:T(128)}, u32[]{:S(2)}) copy-start(f32[4]{0:T(128)} %param.15) | copy-start | bytes 52
  30.3 71.0 %copy-start.4 = (f32[128]{0:T(128)S(1)}, f32[128]{0:T(128)}, u32[]{:S(2)}) copy-start(f32[128]{0:T(128)} %param.16) | copy-start | bytes 1540
  30.3 71.0 %copy-start.1 = (bf16[512,512]{1,0:T(8,128)(2,1)S(1)}, bf16[512,512]{1,0:T(8,128)(2,1)}, u32[]{:S(2)}) copy-start(bf16[512,512]{1,0:T(8,128)(2,1)} %param.17) | copy-start | bytes 1572868
